TPU v7x, 32 devices: a whole 2x2x4 slice. The times are simulated.
32 devices in a mesh: ep: 16 (over z, y, x), tp: 2 (over core).
Axes of the slice: x: 2, y: 2, z: 4, core: 2. Of those that a mesh axis runs over, the one named last changes fastest.
Arguments:
- tokens: bfloat16 [6144, 3072], P('ep', 'tp'), may hold values from -6 to 6
- cotangent: bfloat16 [6144, 3072], P('ep', 'tp'), may hold values from -6 to 6
- experts: int32 [6144, 2], P('ep'), may hold values from 0 to 15, all different within a row; in each aligned block of 384 rows (0 to 383, 384 to 767, ...) at most 72 rows name the same one
- gate: float32 [6144, 2], P('ep'), may hold values from 0.2 to 1
- w_gate: bfloat16 [16, 3072, 768], P('ep', None, 'tp'), may hold values from -0.109375 to 0.109375
- w_up: bfloat16 [16, 3072, 768], P('ep', None, 'tp'), may hold values from -0.109375 to 0.109375
- w_down: bfloat16 [16, 768, 3072], P('ep', 'tp'), may hold values from -0.21875 to 0.21875
Outputs:
- token_grad: bfloat16 [6144, 3072], P('ep', 'tp')
- gate_grad: float32 [6144, 2], P('ep')
- gate_weight_grad: bfloat16 [16, 3072, 768], P('ep', None, 'tp')
- up_weight_grad: bfloat16 [16, 3072, 768], P('ep', None, 'tp')
- down_weight_grad: bfloat16 [16, 768, 3072], P('ep', 'tp')
- gate_row_norms: float32 [16, 3072], P('ep')
- up_row_norms: float32 [16, 3072], P('ep')
- down_row_norms: float32 [16, 768], P('ep', 'tp')
Inputs may be any that keep to these rules, and one draw needn't show every extreme that they name: A row names 2 different experts. In each aligned block of 384 rows (the rows of one index of ep) no expert is named by more than 72 rows, a bound that some block reaches.
All inputs are finite; a program needn't handle non-finite values.
Results may differ from a plain program's by a relative error of at most 0.008.
Values may be sent and summed in bfloat16 or wider, within the bound.
A program may use at most 128 MiB of HBM per device.

v0:
```python
import functools
import jax
import jax.numpy as jnp
from jax import lax
from jax.experimental import pallas as pl
from jax.experimental.pallas import tpu as pltpu
from jax.sharding import PartitionSpec as P

F32 = jnp.float32
BF16 = jnp.bfloat16
LAST = (((1,), (1,)), ((), ()))
ROWS = (((0,), (0,)), ((), ()))
OWN = 0


def slots_of(routes, groups, cap):
    rows = routes.shape[1]
    ids = lax.broadcasted_iota(jnp.int32, (groups, rows), 0)
    hits = [routes[k][None, :] == ids for k in range(routes.shape[0])]
    named = sum(h.astype(F32) for h in hits).astype(BF16)
    before = (
        lax.broadcasted_iota(jnp.int32, (rows, rows), 0)
        < lax.broadcasted_iota(jnp.int32, (rows, rows), 1)
    ).astype(BF16)
    rank = jnp.dot(named, before, preferred_element_type=F32)
    return jnp.stack(
        [routes[k] * cap + jnp.sum(jnp.where(h, rank, 0.0), axis=0).astype(jnp.int32) for k, h in enumerate(hits)]
    )


def wide(width):
    for step in (512, 384, 256, 128):
        if width % step == 0:
            return step
    return width


def forward_kernel(
    n, cap, tok_ref, cot_ref, meta_ref, tok_out, cot_out,
    held, relay, hmeta, rmeta, snd, rows, pick, slot_gate,
    held_send, held_recv, relay_send, relay_recv, pass_send, meta_sem,
    own_send, own_recv, far_send, far_recv, pair_send, pair_recv, out_sem,
):
    rows_t, width = tok_ref.shape
    half_n, quarter = n // 2, n // 4
    me, core = lax.axis_index("ep"), lax.axis_index("tp")
    plane, xy = me // quarter, me % quarter
    side, spot = me // half_n, me % half_n
    outer = jnp.logical_or(plane == 0, plane == 3)
    inner = jnp.logical_not(outer)
    cross = jnp.where(plane == 1, 2, 1) * quarter + xy
    own_inner = (1 + side) * quarter + xy
    near_base = (2 - side) * quarter
    far_base = 3 * (1 - side) * quarter
    columns = pl.ds(pl.multiple_of(core * width, width), width)
    source = (tok_ref, cot_ref)
    blocks = half_n * cap

    def remote(src, dst, send, recv, ep, tp=None):
        return pltpu.make_async_remote_copy(
            src_ref=src, dst_ref=dst, send_sem=send, recv_sem=recv,
            device_id={"ep": ep, "tp": core if tp is None else tp},
            device_id_type=pl.DeviceIdType.MESH,
        )

    barrier = pltpu.get_barrier_semaphore()

    def greet(ep, tp):
        pl.semaphore_signal(barrier, inc=1, device_id={"ep": ep, "tp": tp}, device_id_type=pl.DeviceIdType.MESH)

    for s in range(1, half_n):
        greet(side * half_n + (spot + s) % half_n, core)
    greet(me, 1 - core)

    @pl.when(inner)
    def _():
        greet(cross, core)
        pl.semaphore_wait(barrier, half_n + 1)

    @pl.when(outer)
    def _():
        pl.semaphore_wait(barrier, half_n)

    def near_copy(a):
        return remote(source[a], held.at[0, a], held_send.at[0, a], held_recv.at[0, a], cross)

    def relay_copy(a):
        return remote(source[a], relay.at[a], relay_send.at[a], relay_recv.at[a], own_inner)

    def pass_copy(a):
        return remote(relay.at[a], held.at[1, a], held_send.at[1, a], held_recv.at[1, a], cross)

    near_meta = remote(meta_ref, hmeta.at[0], meta_sem.at[0], meta_sem.at[1], cross)
    relay_meta = remote(meta_ref, rmeta, meta_sem.at[2], meta_sem.at[3], own_inner)
    pass_meta = remote(rmeta, hmeta.at[1], meta_sem.at[4], meta_sem.at[5], cross)

    def own_copy(a, s):
        target = (spot + s) % half_n
        return remote(
            snd.at[OWN, a, target], rows.at[a, me, :, columns],
            own_send.at[a, s], own_recv.at[a, s], side * half_n + target,
        )

    def far_copy(b, a, s, out):
        target = (xy + s) % quarter
        plane_to = 3 * side if out else 1 + side
        base = near_base if b == 0 else far_base
        return remote(
            snd.at[1 + b, a, (plane_to % 2) * quarter + target], rows.at[a, base + xy, :, columns],
            far_send.at[b, a, int(out), s], far_recv.at[b, a, s], plane_to * quarter + target,
        )

    def pair_copy(a, base, count, slot):
        block = rows.at[a, pl.ds(base, count), :, columns]
        return remote(block, block, pair_send.at[a, slot], pair_recv.at[a, slot], me, 1 - core)

    def make_pick(b, table):
        slot = table[0:2, :].astype(jnp.int32) - side * blocks
        ids = lax.broadcasted_iota(jnp.int32, (blocks, rows_t), 0)
        match = [slot[k:k + 1, :] == ids for k in range(2)]
        pick[b] = sum(m.astype(F32) for m in match).astype(BF16)
        slot_gate[b] = sum(
            jnp.sum(jnp.where(m, table[2 + k:3 + k, :], 0.0), axis=1, keepdims=True) for k, m in enumerate(match)
        )

    step = wide(width)

    def fill(b, a, src):
        @pl.loop(0, width // step)
        def _(c):
            cols = pl.ds(pl.multiple_of(c * step, step), step)
            block = jnp.dot(pick[b], src[:, cols], preferred_element_type=F32)
            if a == 1:
                block = block * slot_gate[b]
            snd[b, a, :, :, cols] = block.astype(BF16).reshape(half_n, cap, step)

    def place(b, a, group, where):
        rows[a, group, :, columns] = snd[b, a, where]

    @pl.when(inner)
    def _():
        near_meta.start()
        near_copy(0).start()
        near_copy(1).start()

    @pl.when(outer)
    def _():
        relay_meta.start()
        relay_copy(0).start()

    make_pick(OWN, meta_ref)
    for a in range(2):
        if a == 1:
            @pl.when(outer)
            def _():
                relay_copy(1).start()
        fill(OWN, a, source[a])
        for s in range(half_n - 1, 0, -1):
            own_copy(a, s).start()
        place(OWN, a, me, spot)

    def hand_on(b, a):
        fill(1 + b, a, held.at[b, a])
        for s in range(quarter):
            far_copy(b, a, s, True).start()
        for s in range(1, quarter):
            far_copy(b, a, s, False).start()
        place(1 + b, a, (near_base if b == 0 else far_base) + xy, (1 - side) * quarter + xy)

    def own_arrived(a):
        for s in range(1, half_n):
            own_copy(a, s).wait_recv()
        pair_copy(a, side * half_n, half_n, 0).start()

    def far_arrived(b, a):
        for s in range(1, quarter):
            far_copy(b, a, s, False).wait_recv()

        @pl.when(outer)
        def _():
            far_copy(b, a, 0, True).wait_recv()

        pair_copy(a, near_base if b == 0 else far_base, quarter, 1 + b).start()

    @pl.when(inner)
    def _():
        near_meta.wait_recv()
        relay_meta.wait_recv()
        pass_meta.start()
        make_pick(1, hmeta.at[0])
        relay_copy(0).wait_recv()
        pass_copy(0).start()
        near_copy(0).wait_recv()
        hand_on(0, 0)
        near_copy(1).wait_recv()
        hand_on(0, 1)
        pass_meta.wait_recv()
        make_pick(2, hmeta.at[1])
        relay_copy(1).wait_recv()
        pass_copy(1).start()
        pass_copy(0).wait_recv()
        hand_on(1, 0)

    own_arrived(0)
    far_arrived(0, 0)
    own_arrived(1)
    far_arrived(0, 1)

    @pl.when(inner)
    def _():
        pass_copy(1).wait_recv()
        hand_on(1, 1)

    far_arrived(1, 0)

    far_arrived(1, 1)

    spans = ((side * half_n, half_n), (near_base, quarter), (far_base, quarter))
    for a in range(2):
        for slot, (base, count) in enumerate(spans):
            pair_copy(a, base, count, slot).wait()
    outs = [pltpu.make_async_copy(rows.at[a], (tok_out, cot_out)[a], out_sem.at[a]) for a in range(2)]
    for o in outs:
        o.start()
    for a in range(2):
        for s in range(1, half_n):
            own_copy(a, s).wait_send()

    @pl.when(inner)
    def _():
        near_meta.wait_send()
        pass_meta.wait_send()
        for a in range(2):
            near_copy(a).wait_send()
            pass_copy(a).wait_send()
            for b in range(2):
                for s in range(quarter):
                    far_copy(b, a, s, True).wait_send()
                for s in range(1, quarter):
                    far_copy(b, a, s, False).wait_send()

    @pl.when(outer)
    def _():
        relay_meta.wait_send()
        for a in range(2):
            relay_copy(a).wait_send()

    for o in outs:
        o.wait()


def forward(n, cap, tokens, cotangent, meta):
    rows_t, width = tokens.shape
    half_n, quarter = n // 2, n // 4
    shape = jax.ShapeDtypeStruct((n, cap, 2 * width), BF16)
    dma = pltpu.SemaphoreType.DMA
    vm = pl.BlockSpec(memory_space=pltpu.VMEM)
    return pl.pallas_call(
        functools.partial(forward_kernel, n, cap),
        out_shape=(shape, shape),
        in_specs=[vm] * 3,
        out_specs=[pl.BlockSpec(memory_space=pl.ANY)] * 2,
        scratch_shapes=[
            pltpu.VMEM((2, 2, rows_t, width), BF16),
            pltpu.VMEM((2, rows_t, width), BF16),
            pltpu.VMEM((2,) + meta.shape, F32),
            pltpu.VMEM(meta.shape, F32),
            pltpu.VMEM((3, 2, half_n, cap, width), BF16),
            pltpu.VMEM((2, n, cap, 2 * width), BF16),
            pltpu.VMEM((3, half_n * cap, rows_t), BF16),
            pltpu.VMEM((3, half_n * cap, 1), F32),
            dma((2, 2)), dma((2, 2)), dma((2,)), dma((2,)), dma((2,)), dma((6,)),
            dma((2, half_n)), dma((2, half_n)), dma((2, 2, 2, quarter)), dma((2, 2, quarter)),
            dma((2, 3)), dma((2, 3)), dma((2,)),
        ],
        compiler_params=pltpu.CompilerParams(
            collective_id=0, has_side_effects=True, vmem_limit_bytes=60 * 1024 * 1024
        ),
        cost_estimate=pl.CostEstimate(flops=10**9, bytes_accessed=10**8, transcendentals=0),
    )(tokens, cotangent, meta)


def per_device(tokens, cotangent, experts, gate, w_gate, w_up, w_down):
    groups = lax.axis_size("ep")
    tok_rows, top = experts.shape
    cap = 3 * tok_rows * top // (2 * groups)
    cap = (cap + 7) // 8 * 8
    total = groups * cap
    half = tokens.shape[1]
    core = lax.axis_index("tp")
    swap = [(0, 1), (1, 0)]
    slot = slots_of(experts.T, groups, cap)
    gate_t = gate.T
    meta = jnp.concatenate([slot.astype(F32), gate_t, jnp.zeros((4, tok_rows), F32)], axis=0)
    rows_in, rows_cot = forward(groups, cap, tokens, cotangent, meta)
    rows_in, rows_cot = rows_in.reshape(total, 2 * half), rows_cot.reshape(total, 2 * half)
    slot_ids = lax.broadcasted_iota(jnp.int32, (total, tok_rows), 0)
    match = [slot[k][None, :] == slot_ids for k in range(top)]
    pick = sum(m.astype(F32) for m in match).astype(BF16)

    def exchange(x):
        y = lax.all_to_all(x.reshape(groups, cap, -1), "ep", split_axis=0, concat_axis=0, tiled=True)
        return y.reshape(total, -1)

    w_in = jnp.concatenate([w_gate[0], w_up[0]], axis=1)
    hid = w_gate.shape[2]
    w_mine = lax.dynamic_slice_in_dim(w_in, core * half, half, 0)
    w_other = lax.dynamic_slice_in_dim(w_in, (1 - core) * half, half, 0)
    pre = jnp.dot(rows_in, w_in, preferred_element_type=F32)
    hidden_grad = lax.dot_general(rows_cot, w_down[0], LAST, preferred_element_type=F32)
    gate_pre, up_pre = pre[:, :hid], pre[:, hid:]
    sigma = jax.nn.sigmoid(gate_pre)
    active = gate_pre * sigma
    hidden = (active * up_pre).astype(BF16)
    product_part = jnp.sum(hidden.astype(F32) * hidden_grad, axis=1)
    grads = jnp.concatenate(
        [
            (hidden_grad * up_pre * sigma * (1.0 + gate_pre * (1.0 - sigma))).astype(BF16),
            (hidden_grad * active).astype(BF16),
        ],
        axis=1,
    )
    part_other = lax.dot_general(grads, w_other, LAST, preferred_element_type=F32).astype(BF16)
    arrived = lax.ppermute(part_other, "tp", swap)
    part_mine = lax.dot_general(grads, w_mine, LAST, preferred_element_type=F32)
    row_grads = (part_mine + arrived.astype(F32)).astype(BF16)
    high = product_part.astype(BF16)
    low = (product_part - high.astype(F32)).astype(BF16)
    lane = lax.broadcasted_iota(jnp.int32, (total, 128), 1)
    spare = jnp.where(lane == 0, high[:, None], jnp.where(lane == 1, low[:, None], jnp.zeros((), BF16)))
    row_grads = jnp.concatenate([row_grads, spare], axis=1)
    back = exchange(row_grads)

    rows_in, grads, rows_cot, hidden, row_grads = lax.optimization_barrier(
        (rows_in, grads, rows_cot, hidden, row_grads)
    )
    gate_sum = lax.dot_general(rows_in, grads[:, :hid], ROWS, preferred_element_type=F32)
    up_sum = lax.dot_general(rows_in, grads[:, hid:], ROWS, preferred_element_type=F32)
    down_sum = lax.dot_general(hidden, rows_cot, ROWS, preferred_element_type=F32)
    in_norms = jnp.stack([jnp.sum(gate_sum * gate_sum, axis=1), jnp.sum(up_sum * up_sum, axis=1)])
    down_norms = jnp.sum(down_sum * down_sum, axis=1)
    in_norms = in_norms + lax.ppermute(in_norms, "tp", swap)
    pair = lax.dot_general(
        back[:, half:], jnp.concatenate([match[k] for k in range(top)], axis=1).astype(BF16), ROWS,
        preferred_element_type=F32,
    )
    route_products = (pair[0] + pair[1]).reshape(top, tok_rows)
    route_products = route_products + lax.ppermute(route_products, "tp", swap)
    gate_grad = (route_products.astype(BF16).astype(F32) / gate_t).T
    token_grad = lax.dot_general(pick, back[:, :half], ROWS, preferred_element_type=F32).astype(BF16)
    return (
        token_grad,
        gate_grad,
        gate_sum.astype(BF16)[None],
        up_sum.astype(BF16)[None],
        down_sum.astype(BF16)[None],
        in_norms[0][None],
        in_norms[1][None],
        down_norms[None],
    )


def solution(mesh):
    placed = (
        P("ep", "tp"),
        P("ep", "tp"),
        P("ep", None),
        P("ep", None),
        P("ep", None, "tp"),
        P("ep", None, "tp"),
        P("ep", "tp", None),
    )
    return jax.shard_map(
        per_device,
        mesh=mesh,
        in_specs=placed,
        out_specs=(
            P("ep", "tp"),
            P("ep", None),
            P("ep", None, "tp"),
            P("ep", None, "tp"),
            P("ep", "tp", None),
            P("ep", None),
            P("ep", None),
            P("ep", "tp"),
        ),
        check_vma=False,
    )
```

profile of v0, /device:TPU:15, one launch (start us, length us, event | category | flops | bytes accessed | tf_op | source)
XLA Modules:
  0.0 281.3 jit_solution(16335387172318150941)
XLA Ops:
  0.6 0.0 copy-start
  0.7 0.9 slice_reduce_fusion.1
  1.5 0.2 select_reduce_fusion.1
  1.7 0.8 fusion.38
  2.5 0.1 pad.12.clone
  2.6 1.4 maximum_maximum_fusion.meta_ref
  4.0 128.6 %shard_map.134 = (bf16[16,72,3072]{2,1,0:T(8,128)(2,1)}, bf16[16,72,3072]{2,1,0:T(8,128)(2,1)}) custom-call(bf16[384,1536]{1,0:T(8,128)(2,1)} %tok_ref.1, bf16[384,1536]{1,0:T(8,128)(2,1)} %cot_ref.1, f32[8,384]{1,0:T(8,128)} %maximum_maximum_fusion.meta_ref), custom_call_target="tpu_custom_call" | custom-call | flops 1000000000 | bytes 100000000 | tf_op jit(solution)/shard_map/pallas_call | solution.py:258
  132.5 0.0 copy-start.5
  132.6 10.8 %fusion = f32[1152,768]{0,1:T(8,128)S(1)} fusion(bf16[1152,3072]{1,0:T(8,128)(2,1)} %bitcast.48, bf16[3072,384]{1,0:T(8,128)(2,1)} %bitcast.38, bf16[3072,384]{1,0:T(8,128)(2,1)} %bitcast.41), kind=kOutput, calls=%fused_computation.7 | convolution fusion | flops 5445255168 | bytes 15335424 | tf_op jit(solution)/shard_map/dot_general | solution.py:309
  143.3 0.0 copy-done
  143.3 0.0 copy-done.5
  143.3 0.0 copy-start.3
  143.4 0.0 copy-start.4
  143.4 4.7 %multiply_reduce_fusion.3 = (f32[1152]{0:T(1024)S(1)}, bf16[1152,384]{0,1:T(8,128)(2,1)}, bf16[1152,384]{0,1:T(8,128)(2,1)S(1)}, bf16[1152,384]{0,1:T(8,128)(2,1)S(1)}) fusion(f32[1152,768]{0,1:T(8,128)S(1)} %fusion, bf16[1152,3072]{1,0:T(8,128)(2,1)S(1)} %bitcast.44, bf16[1,384,3072]{2,1,0:T(8,128)(2,1)S(1)} %copy-done), kind=kOutput, calls=%fused_computation.28 | convolution fusion | flops 2725870592 | bytes 15634944 | tf_op jit(solution)/shard_map/dot_general | solution.py:310
  148.1 0.0 copy-start.1
  148.1 0.0 copy-done.3
  148.1 0.0 copy-done.4
  148.1 4.5 %convolution_convert_fusion = bf16[1152,1536]{1,0:T(8,128)(2,1)} fusion(s32[]{:T(128)S(6)} %select_n.24, bf16[3072,384]{1,0:T(8,128)(2,1)S(1)} %bitcast.43, bf16[3072,384]{1,0:T(8,128)(2,1)S(1)} %bitcast.40, bf16[1152,384]{0,1:T(8,128)(2,1)S(1)} %get-tuple-element.41, bf16[1152,384]{0,1:T(8,128)(2,1)S(1)} %get-tuple-element.40), kind=kOutput, calls=%fused_computation | convolution fusion | flops 2727936000 | bytes 10027012 | tf_op jit(solution)/shard_map/dot_general | solution.py:323
  152.6 0.0 copy-done.1
  152.6 0.2 collective-permute-start
  152.8 0.4 select_select_fusion
  153.2 6.0 %collective-permute-done = bf16[1152,1536]{1,0:T(8,128)(2,1)} collective-permute-done((bf16[1152,1536]{1,0:T(8,128)(2,1)}, bf16[1152,1536]{1,0:T(8,128)(2,1)}, u32[]{:S(2)}, u32[]{:S(2)}) %collective-permute-start) | collective-permute-done | bytes 3538976 | tf_op jit(solution)/shard_map/ppermute | solution.py:324
  159.2 6.0 %add_convert_fusion = bf16[1152,1536]{1,0:T(8,128)(2,1)S(1)} fusion(bf16[1152,1536]{1,0:T(8,128)(2,1)} %collective-permute-done, s32[]{:T(128)S(6)} %select_n.23, bf16[3072,384]{1,0:T(8,128)(2,1)} %bitcast.42, bf16[3072,384]{1,0:T(8,128)(2,1)} %bitcast.39, bf16[1152,384]{0,1:T(8,128)(2,1)} %copy-done.1, bf16[1152,384]{0,1:T(8,128)(2,1)S(1)} %get-tuple-element.40), kind=kOutput, calls=%fused_computation.1 | convolution fusion | flops 2731474944 | bytes 13565956 | tf_op jit(solution)/shard_map/dot_general | solution.py:325
  165.2 2.1 pad_maximum_fusion.2
  167.3 18.2 %all-to-all-start = ((bf16[16,72,1664]{2,1,0:T(8,128)(2,1)}), bf16[16,72,1664]{2,1,0:T(8,128)(2,1)}, u32[]{:S(2)}, u32[]{:S(2)}) async-start(bf16[16,72,1664]{2,1,0:T(8,128)(2,1)} %bitcast.30), calls=%async_computation | async-start | bytes 7667712 | tf_op jit(solution)/shard_map/all_to_all | solution.py:302
  185.6 0.0 slice-start.2
  185.6 1.5 pad_maximum_fusion.3
  187.0 0.5 iota_compare_fusion
  187.6 0.0 slice-start.3
  187.6 0.0 slice-start
  187.6 7.6 %multiply_reduce_fusion.1 = (f32[3072]{0:T(1024)S(1)}, bf16[1,3072,384]{1,2,0:T(8,128)(2,1)}) fusion(bf16[1152,3072]{1,0:T(8,128)(2,1)} %bitcast.49, bf16[1152,768]{0,1:T(8,128)(2,1)S(1)} %pad_maximum_fusion.3), kind=kOutput, calls=%fused_computation.9 | convolution fusion | flops 2721444864 | bytes 10334208 | tf_op jit(solution)/shard_map/dot_general | solution.py:338
  195.2 0.0 slice-done.2
  195.2 0.0 slice-done.3
  195.2 0.0 slice-start.1
  195.2 0.0 copy-start.6
  195.2 4.6 %multiply_reduce_fusion.2 = (f32[3072]{0:T(1024)S(1)}, bf16[1,3072,384]{1,2,0:T(8,128)(2,1)}) fusion(bf16[1152,3072]{1,0:T(8,128)(2,1)S(1)} %bitcast.52, bf16[1152,768]{0,1:T(8,128)(2,1)S(1)} %pad_maximum_fusion.3), kind=kOutput, calls=%fused_computation.10 | convolution fusion | flops 2721444864 | bytes 10334208 | tf_op jit(solution)/shard_map/dot_general | solution.py:337
  199.9 0.8 collective-permute-start.2
  200.7 0.0 slice-done
  200.7 0.0 slice-done.1
  200.7 0.0 copy-done.6
  200.7 4.5 %multiply_reduce_fusion = (f32[384]{0:T(512)S(1)}, bf16[1,384,3072]{2,1,0:T(8,128)(2,1)}) fusion(bf16[1152,384]{0,1:T(8,128)(2,1)S(1)} %copy-done.6, bf16[1152,3072]{1,0:T(8,128)(2,1)S(1)} %bitcast.47), kind=kOutput, calls=%fused_computation.8 | convolution fusion | flops 2721447424 | bytes 10323456 | tf_op jit(solution)/shard_map/dot_general | solution.py:339
  205.2 0.6 broadcast_in_dim.50
  205.8 4.3 %copy.16 = bf16[1,3072,384]{2,1,0:T(8,128)(2,1)} copy(bf16[1,3072,384]{1,2,0:T(8,128)(2,1)} %get-tuple-element.47) | data formatting | bytes 4718592
  210.1 4.3 %copy.15 = bf16[1,3072,384]{2,1,0:T(8,128)(2,1)} copy(bf16[1,3072,384]{1,2,0:T(8,128)(2,1)} %get-tuple-element.45) | data formatting | bytes 4718592
  214.3 0.0 collective-permute-done.2
  214.4 0.6 fusion.39
  215.0 58.0 %all-to-all-done = bf16[16,72,1664]{2,1,0:T(8,128)(2,1)} async-done(((bf16[16,72,1664]{2,1,0:T(8,128)(2,1)}), bf16[16,72,1664]{2,1,0:T(8,128)(2,1)}, u32[]{:S(2)}, u32[]{:S(2)}) %all-to-all-start) | async-done | bytes 3833888 | tf_op jit(solution)/shard_map/all_to_all | solution.py:302
  273.0 1.6 fusion.3
  274.6 0.0 copy-start.2
  274.6 1.3 collective-permute-start.1
  276.0 4.8 %fusion.7 = bf16[384,1536]{1,0:T(8,128)(2,1)} fusion(bf16[1152,1664]{1,0:T(8,128)(2,1)} %bitcast.8, s32[384]{0:T(512)S(1)} %get-tuple-element.34, s32[384]{0:T(512)S(1)} %get-tuple-element.50), kind=kOutput, calls=%fused_computation.18 | convolution fusion | flops 1362198528 | bytes 4721664 | tf_op jit(solution)/shard_map/dot_general | solution.py:350
  280.7 0.0 collective-permute-done.1
  280.7 0.0 copy-done.2
  280.7 0.6 fusion.29
  (12 shorter events, 0.1 us)
Async XLA Ops:
  0.6 142.7 %copy-start = (bf16[1,384,3072]{2,1,0:T(8,128)(2,1)S(1)}, bf16[1,384,3072]{2,1,0:T(8,128)(2,1)}, u32[]{:S(2)}) copy-start(bf16[1,384,3072]{2,1,0:T(8,128)(2,1)} %param.13) | copy-start | bytes 7077892
  132.5 10.8 %copy-start.5 = (bf16[16,72,3072]{2,1,0:T(8,128)(2,1)S(1)}, bf16[16,72,3072]{2,1,0:T(8,128)(2,1)}, u32[]{:S(2)}) copy-start(bf16[16,72,3072]{2,1,0:T(8,128)(2,1)} %get-tuple-element.14) | copy-start | bytes 21233668
  143.3 4.8 %copy-start.3 = (bf16[1,3072,384]{2,1,0:T(8,128)(2,1)S(1)}, bf16[1,3072,384]{2,1,0:T(8,128)(2,1)}, u32[]{:S(2)}) copy-start(bf16[1,3072,384]{2,1,0:T(8,128)(2,1)} %param.12) | copy-start | bytes 7077892
  143.4 4.8 %copy-start.4 = (bf16[1,3072,384]{2,1,0:T(8,128)(2,1)S(1)}, bf16[1,3072,384]{2,1,0:T(8,128)(2,1)}, u32[]{:S(2)}) copy-start(bf16[1,3072,384]{2,1,0:T(8,128)(2,1)} %param.11) | copy-start | bytes 7077892
  148.1 4.5 %copy-start.1 = (bf16[1152,384]{0,1:T(8,128)(2,1)}, bf16[1152,384]{0,1:T(8,128)(2,1)S(1)}, u32[]{:S(2)}) copy-start(bf16[1152,384]{0,1:T(8,128)(2,1)S(1)} %get-tuple-element.41) | copy-start | bytes 2654212
  152.6 6.6 %collective-permute-start = (bf16[1152,1536]{1,0:T(8,128)(2,1)}, bf16[1152,1536]{1,0:T(8,128)(2,1)}, u32[]{:S(2)}, u32[]{:S(2)}) collective-permute-start(bf16[1152,1536]{1,0:T(8,128)(2,1)} %convolution_convert_fusion), channel_id=1, source_target_pairs={{0,1},{1,0},{2,3},{3,2},{4,5},{5,4},{6,7},{7,6},{8,9},{9,8},{10,11... | collective-permute-start | bytes 10616840 | tf_op jit(solution)/shard_map/ppermute | solution.py:324
  167.3 105.7 %all-to-all-start = ((bf16[16,72,1664]{2,1,0:T(8,128)(2,1)}), bf16[16,72,1664]{2,1,0:T(8,128)(2,1)}, u32[]{:S(2)}, u32[]{:S(2)}) async-start(bf16[16,72,1664]{2,1,0:T(8,128)(2,1)} %bitcast.30), calls=%async_computation | async-start | bytes 7667712 | tf_op jit(solution)/shard_map/all_to_all | solution.py:302
  185.6 9.6 %slice-start.2 = ((s8[7077888]{0:T(1024)(128)(4,1)}), s8[4194304]{0:T(1024)(128)(4,1)S(1)}, s32[]{:S(2)}) async-start(s8[7077888]{0:T(1024)(128)(4,1)} %bitcast.50), calls=%async_computation.3 | async-start | bytes 8388608
  187.6 7.6 %slice-start.3 = ((s8[7077888]{0:T(1024)(128)(4,1)}), s8[2883584]{0:T(1024)(128)(4,1)S(1)}, s32[]{:S(2)}) async-start(s8[7077888]{0:T(1024)(128)(4,1)} %bitcast.50), calls=%async_computation.4 | async-start | bytes 5767168
  187.6 13.1 %slice-start = ((s8[7077888]{0:T(1024)(128)(4,1)}), s8[4194304]{0:T(1024)(128)(4,1)S(1)}, s32[]{:S(2)}) async-start(s8[7077888]{0:T(1024)(128)(4,1)} %bitcast.45), calls=%async_computation.1 | async-start | bytes 8388608
  195.2 5.4 %slice-start.1 = ((s8[7077888]{0:T(1024)(128)(4,1)}), s8[2883584]{0:T(1024)(128)(4,1)S(1)}, s32[]{:S(2)}) async-start(s8[7077888]{0:T(1024)(128)(4,1)} %bitcast.45), calls=%async_computation.2 | async-start | bytes 5767168
  195.2 5.4 %copy-start.6 = (bf16[1152,384]{0,1:T(8,128)(2,1)S(1)}, bf16[1152,384]{0,1:T(8,128)(2,1)}, u32[]{:S(2)}) copy-start(bf16[1152,384]{0,1:T(8,128)(2,1)} %get-tuple-element.18) | copy-start | bytes 2654212
  199.9 14.4 %collective-permute-start.2 = (f32[2,3072]{1,0:T(2,128)S(1)}, f32[2,3072]{1,0:T(2,128)S(1)}, u32[]{:S(2)}, u32[]{:S(2)}) collective-permute-start(f32[2,3072]{1,0:T(2,128)S(1)} %pad_maximum_fusion.4), channel_id=1, source_target_pairs={{0,1},{1,0},{2,3},{3,2},{4,5},{5,4},{6,7},{7,6},{8,9},{9,8},{10,11... | collective-permute-start | bytes 73736 | tf_op jit(solution)/shard_map/ppermute | solution.py:342
  274.6 6.1 %copy-start.2 = (f32[384,2]{0,1:T(2,128)S(1)}, f32[384,2]{0,1:T(2,128)}, u32[]{:S(2)}) copy-start(f32[384,2]{0,1:T(2,128)} %param.10) | copy-start | bytes 9220
  274.6 6.1 %collective-permute-start.1 = (f32[2,384]{1,0:T(2,128)S(1)}, f32[2,384]{1,0:T(2,128)S(1)}, u32[]{:S(2)}, u32[]{:S(2)}) collective-permute-start(f32[2,384]{1,0:T(2,128)S(1)} %add.52), channel_id=1, source_target_pairs={{0,1},{1,0},{2,3},{3,2},{4,5},{5,4},{6,7},{7,6},{8,9},{9,8},{10,11... | collective-permute-start | bytes 9224 | tf_op jit(solution)/shard_map/ppermute | solution.py:348
where the time goes:
time: 282 us; the launch traced here: 281 us
  Pallas kernels  129 us (46%)
  waiting for transfers between devices  64.1 us (23%)
  matrix products  49.3 us (17%)
  starting transfers between devices  20.5 us (7%)
  local copies, waits for them, and re-layouts  10.7 us (4%)
  other arithmetic  7.32 us (3%)
    pallas_call x1, Pallas kernels, forward(): pl.pallas_call(functools.partial(forward_kernel, n, cap), out_shape=(shap...  129 us
    all_to_all x1, waiting for transfers between devices, exchange(): lax.all_to_all(x.reshape(groups, cap, -1), 'ep', split_axis=0, concat_axi...  58 us
    all_to_all x1, starting transfers between devices, exchange(): lax.all_to_all(x.reshape(groups, cap, -1), 'ep', split_axis=0, concat_axi...  18.2 us
    dot_general x1, matrix products, per_device(): pre = jnp.dot(rows_in, w_in, preferred_element_type=F32)  10.8 us
    unnamed x24, local copies, waits for them, and re-layouts  8.59 us
    dot_general x1, matrix products, per_device(): lax.dot_general(rows_in, grads[:, hid:], ROWS, preferred_element_type=F32)  7.62 us
    ppermute x1, waiting for transfers between devices, per_device(): arrived = lax.ppermute(part_other, 'tp', swap)  6.03 us
    dot_general x1, matrix products, per_device(): part_mine = lax.dot_general(grads, w_mine, LAST, preferred_element_type=F32)  5.98 us
  transfers between devices with their start and end apart: 4, of which 2 were waited for; matrix products, arithmetic and copies ran while one was open for 12% of the time, Pallas kernels for 0%

commit v1 on v0

v1 whole, which is shorter than its diff:
```python
import functools
import jax
import jax.numpy as jnp
from jax import lax
from jax.experimental import pallas as pl
from jax.experimental.pallas import tpu as pltpu
from jax.sharding import PartitionSpec as P

F32 = jnp.float32
BF16 = jnp.bfloat16
LAST = (((1,), (1,)), ((), ()))
ROWS = (((0,), (0,)), ((), ()))
MESH = pl.DeviceIdType.MESH
VMEM_BYTES = 67043328


def slots_of(routes, groups, cap):
    rows = routes.shape[1]
    ids = lax.broadcasted_iota(jnp.int32, (groups, rows), 0)
    hits = [routes[k][None, :] == ids for k in range(routes.shape[0])]
    named = sum(h.astype(F32) for h in hits).astype(BF16)
    before = (
        lax.broadcasted_iota(jnp.int32, (rows, rows), 0)
        < lax.broadcasted_iota(jnp.int32, (rows, rows), 1)
    ).astype(BF16)
    rank = jnp.dot(named, before, preferred_element_type=F32)
    return jnp.stack(
        [routes[k] * cap + jnp.sum(jnp.where(h, rank, 0.0), axis=0).astype(jnp.int32) for k, h in enumerate(hits)]
    )


def wide(width):
    for step in (512, 384, 256, 128):
        if width % step == 0:
            return step
    return width


def layer_kernel(
    n, cap, tok_ref, cot_ref, meta_ref, w_gate, w_up, w_down,
    tok_out, gate_out, gate_w, up_w, down_w, in_norms, down_norms,
    held, relay, hmeta, rmeta, snd, rows, pick, slot_gate, w_in, w_out, pre, grads, hidden,
    part, arr, back_own, back_far, far_part, prod, norms, col_norm,
    held_send, held_recv, relay_send, relay_recv, meta_sem,
    own_send, own_recv, far_send, far_recv, pair_send, pair_recv, w_sem,
    part_send, part_recv, bo_send, bo_recv, bf_send, bf_recv, fp_send, fp_recv,
    prod_send, prod_recv, pp_sem, norm_sem, out_sem, tok_sem,
):
    rows_t, width = tok_ref.shape
    hid = w_down.shape[1]
    half_n, quarter = n // 2, n // 4
    unit = quarter * cap
    me, core = lax.axis_index("ep"), lax.axis_index("tp")
    plane, xy = me // quarter, me % quarter
    side, spot = me // half_n, me % half_n
    outer = jnp.logical_or(plane == 0, plane == 3)
    inner = jnp.logical_not(outer)
    cross = jnp.where(plane == 1, 2, 1) * quarter + xy
    own_inner = (1 + side) * quarter + xy
    own_base = side * half_n
    near_base = (2 - side) * quarter
    far_base = 3 * (1 - side) * quarter
    bases = (near_base, far_base)
    columns = pl.ds(pl.multiple_of(core * width, width), width)
    source = (tok_ref, cot_ref)
    blocks = half_n * cap
    step = wide(width)
    chunks = width // step
    tiles = hid // 128

    def cols(c):
        return pl.ds(c * step, step)

    def remote(src, dst, send, recv, ep, tp=None):
        return pltpu.make_async_remote_copy(
            src_ref=src, dst_ref=dst, send_sem=send, recv_sem=recv,
            device_id={"ep": ep, "tp": core if tp is None else tp}, device_id_type=MESH,
        )

    loads = []
    for j in range(tiles):
        for k, w in enumerate((w_gate, w_up)):
            loads.append(pltpu.make_async_copy(
                w.at[0, :, pl.ds(j * 128, 128)], w_in.at[:, pl.ds(j * 256 + k * 128, 128)], w_sem.at[len(loads)]
            ))
    loads.append(pltpu.make_async_copy(w_down.at[0], w_out, w_sem.at[len(loads)]))

    barrier = pltpu.get_barrier_semaphore()
    for s in range(1, n):
        pl.semaphore_signal(barrier, inc=1, device_id={"ep": (me + s) % n, "tp": core}, device_id_type=MESH)
    pl.semaphore_signal(barrier, inc=1, device_id={"ep": me, "tp": 1 - core}, device_id_type=MESH)
    pl.semaphore_wait(barrier, n)

    def near_copy(a):
        return remote(source[a], held.at[0, a], held_send.at[0, a], held_recv.at[0, a], cross)

    def relay_copy(a):
        return remote(source[a], relay.at[a], relay_send.at[a], relay_recv.at[a], own_inner)

    def pass_copy(a):
        return remote(relay.at[a], held.at[1, a], held_send.at[1, a], held_recv.at[1, a], cross)

    near_meta = remote(meta_ref, hmeta.at[0], meta_sem.at[0], meta_sem.at[1], cross)
    relay_meta = remote(meta_ref, rmeta, meta_sem.at[2], meta_sem.at[3], own_inner)
    pass_meta = remote(rmeta, hmeta.at[1], meta_sem.at[4], meta_sem.at[5], cross)

    def own_copy(a, s):
        target = (spot + s) % half_n
        return remote(
            snd.at[0, a, target], rows.at[a, me, :, columns],
            own_send.at[a, s], own_recv.at[a, s], own_base + target,
        )

    def far_copy(b, a, s, out):
        target = (xy + s) % quarter
        plane_to = 3 * side if out else 1 + side
        return remote(
            snd.at[1 - b, a, (plane_to % 2) * quarter + target], rows.at[a, bases[b] + xy, :, columns],
            far_send.at[b, a, int(out), s], far_recv.at[b, a, s], plane_to * quarter + target,
        )

    spans = ((own_base, half_n), (near_base, quarter), (far_base, quarter))

    def pair_copy(a, slot):
        block = rows.at[a, pl.ds(*spans[slot]), :, columns]
        return remote(block, block, pair_send.at[a, slot], pair_recv.at[a, slot], me, 1 - core)

    def make_pick(b, table):
        slot = table[0:2, :].astype(jnp.int32) - side * blocks
        ids = lax.broadcasted_iota(jnp.int32, (blocks, rows_t), 0)
        match = [slot[k:k + 1, :] == ids for k in range(2)]
        pick[b] = sum(m.astype(F32) for m in match).astype(BF16)
        slot_gate[b] = sum(
            jnp.sum(jnp.where(m, table[2 + k:3 + k, :], 0.0), axis=1, keepdims=True) for k, m in enumerate(match)
        )

    def fill(b, where, a, src):
        @pl.loop(0, chunks)
        def _(c):
            span = pl.ds(pl.multiple_of(c * step, step), step)
            block = jnp.dot(pick[b], src[:, span], preferred_element_type=F32)
            if a == 1:
                block = block * slot_gate[b]
            snd[where, a, :, :, span] = block.astype(BF16).reshape(half_n, cap, step)

    def hand_on(b, a):
        fill(1 + b, 1 - b, a, held.at[b, a])
        for s in range(quarter):
            far_copy(b, a, s, True).start()
        for s in range(1, quarter):
            far_copy(b, a, s, False).start()
        rows[a, bases[b] + xy, :, columns] = snd[1 - b, a, (1 - side) * quarter + xy]

    def own_arrived(a):
        for s in range(1, half_n):
            own_copy(a, s).wait_recv()
        pair_copy(a, 0).start()

    def far_arrived(b, a):
        for s in range(1, quarter):
            far_copy(b, a, s, False).wait_recv()

        @pl.when(outer)
        def _():
            far_copy(b, a, 0, True).wait_recv()

        pair_copy(a, 1 + b).start()

    def pre_unit(base):
        x = rows[0, pl.ds(base, quarter)].reshape(unit, 2 * width)
        pre[pl.ds(base, quarter)] = jnp.dot(x, w_in[...], preferred_element_type=F32).reshape(quarter, cap, 2 * hid)

    def mid_unit(base):
        x = rows[1, pl.ds(base, quarter)].reshape(unit, 2 * width)
        grad = lax.dot_general(x, w_out[...], LAST, preferred_element_type=F32)
        total = jnp.zeros((unit, 1), F32)
        for j in range(tiles):
            gate_pre = pre[pl.ds(base, quarter), :, j * 256:j * 256 + 128].reshape(unit, 128)
            up_pre = pre[pl.ds(base, quarter), :, j * 256 + 128:j * 256 + 256].reshape(unit, 128)
            g = grad[:, j * 128:(j + 1) * 128]
            sigma = jax.nn.sigmoid(gate_pre)
            active = gate_pre * sigma
            kept = (active * up_pre).astype(BF16)
            total = total + jnp.sum(kept.astype(F32) * g, axis=1, keepdims=True)
            hidden[pl.ds(base, quarter), :, j * 128:(j + 1) * 128] = kept.reshape(quarter, cap, 128)
            one = (g * up_pre * sigma * (1.0 + gate_pre * (1.0 - sigma))).astype(BF16)
            two = (g * active).astype(BF16)
            grads[pl.ds(base, quarter), :, j * 256:j * 256 + 128] = one.reshape(quarter, cap, 128)
            grads[pl.ds(base, quarter), :, j * 256 + 128:j * 256 + 256] = two.reshape(quarter, cap, 128)
        diagonal = lax.broadcasted_iota(jnp.int32, (cap, 128), 0) == lax.broadcasted_iota(jnp.int32, (cap, 128), 1)
        for q in range(quarter):
            line = jnp.sum(jnp.where(diagonal, total[q * cap:(q + 1) * cap], 0.0), axis=0, keepdims=True)
            prod[0, base + q] = jnp.broadcast_to(line, (8, 128))

    def part_copy(kind, c):
        block = pl.ds(*spans[kind])
        return remote(
            part.at[block, :, cols(c)], arr.at[block, :, cols(c)],
            part_send.at[kind, c], part_recv.at[kind, c], me, 1 - core,
        )

    def product(base, c, whose):
        g = grads[pl.ds(base, quarter)].reshape(unit, 2 * hid)
        w = w_in[pl.ds(pl.multiple_of(whose * width + c * step, step), step), :]
        return lax.dot_general(g, w, LAST, preferred_element_type=F32).reshape(quarter, cap, step)

    def unit_bases(kind):
        return (own_base, own_base + quarter) if kind == 0 else (bases[kind - 1],)

    def part_out(kind):
        for c in range(chunks):
            for base in unit_bases(kind):
                part[pl.ds(base, quarter), :, cols(c)] = product(base, c, 1 - core).astype(BF16)
            part_copy(kind, c).start()

    def back_own_copy(c, s):
        target = (spot + s) % half_n
        return remote(
            arr.at[own_base + target, :, cols(c)], back_own.at[spot, :, cols(c)],
            bo_send.at[c, s], bo_recv.at[c, spot], own_base + target,
        )

    def back_far_copy(b, c, s):
        target = (xy + s) % quarter
        return remote(
            arr.at[bases[b] + target, :, cols(c)], back_far.at[b, spot, :, cols(c)],
            bf_send.at[b, c, s], bf_recv.at[b, c, spot], (1 + side) * quarter + target,
        )

    def send_back(kind):
        for c in range(chunks):
            part_copy(kind, c).wait_recv()
            for base in unit_bases(kind):
                here = pl.ds(base, quarter)
                arr[here, :, cols(c)] = (product(base, c, core) + arr[here, :, cols(c)].astype(F32)).astype(BF16)
            if kind == 0:
                for s in range(1, half_n):
                    back_own_copy(c, s).start()
                back_own[spot, :, cols(c)] = arr[me, :, cols(c)]
            else:
                for s in range(1, quarter):
                    back_far_copy(kind - 1, c, s).start()

                @pl.when(outer)
                def _():
                    back_far_copy(kind - 1, c, 0).start()

                @pl.when(inner)
                def _():
                    back_far[kind - 1, spot, :, cols(c)] = arr[bases[kind - 1] + xy, :, cols(c)]

    def far_part_copy(b, c):
        return remote(
            relay.at[b, :, cols(c)], far_part.at[:, cols(c)],
            fp_send.at[b, c], fp_recv.at[c], cross if b == 0 else far_base + xy,
        )

    def combine(b, src, c):
        block = src[:, :, cols(c)].reshape(blocks, step)
        return lax.dot_general(pick[b], block, ROWS, preferred_element_type=F32)

    def far_combine(b):
        for c in range(chunks):
            for s in range(1, half_n):
                other = (spot + s) % half_n
                block = back_far.at[b, other, :, cols(c)]
                remote(block, block, bf_send.at[b, c, 0], bf_recv.at[b, c, other], me, 1 - core).wait_recv()
            relay[b, :, cols(c)] = combine(1 + b, back_far.at[b], c).astype(BF16)
            far_part_copy(b, c).start()

    @pl.when(inner)
    def _():
        near_meta.start()
        near_copy(0).start()
        near_copy(1).start()

    @pl.when(outer)
    def _():
        relay_meta.start()
        relay_copy(0).start()

    for load in loads:
        load.start()
    make_pick(0, meta_ref)
    for a in range(2):
        if a == 1:
            @pl.when(outer)
            def _():
                relay_copy(1).start()
        fill(0, 0, a, source[a])
        for s in range(half_n - 1, 0, -1):
            own_copy(a, s).start()
        rows[a, me, :, columns] = snd[0, a, spot]

    @pl.when(inner)
    def _():
        near_meta.wait_recv()
        relay_meta.wait_recv()
        pass_meta.start()
        make_pick(1, hmeta.at[0])
        relay_copy(0).wait_recv()
        pass_copy(0).start()
        near_copy(0).wait_recv()
        hand_on(0, 0)

    own_arrived(0)

    @pl.when(inner)
    def _():
        near_copy(1).wait_recv()
        hand_on(0, 1)

    far_arrived(0, 0)
    for load in loads:
        load.wait()
    pair_copy(0, 0).wait_recv()

    @pl.loop(0, 2)
    def _(u):
        pre_unit(own_base + u * quarter)

    @pl.when(inner)
    def _():
        pass_meta.wait_recv()
        make_pick(2, hmeta.at[1])
        relay_copy(1).wait_recv()
        pass_copy(1).start()

    pair_copy(0, 1).wait_recv()
    pre_unit(near_base)
    for a in range(2):
        for s in range(1, half_n):
            own_copy(a, s).wait_send()

    @pl.when(inner)
    def _():
        pass_copy(0).wait_recv()
        hand_on(1, 0)

    far_arrived(0, 1)
    pair_copy(1, 1).wait_recv()
    mid_unit(near_base)
    part_out(1)
    own_arrived(1)
    send_back(1)
    pair_copy(1, 0).wait_recv()

    @pl.loop(0, 2)
    def _(u):
        mid_unit(own_base + u * quarter)

    @pl.when(inner)
    def _():
        pass_copy(1).wait_recv()
        hand_on(1, 1)

    far_arrived(1, 0)
    part_out(0)
    pair_copy(0, 2).wait_recv()
    pre_unit(far_base)
    send_back(0)

    @pl.when(inner)
    def _():
        for a in range(2):
            pass_copy(a).wait_send()
        far_combine(0)

    far_arrived(1, 1)
    pair_copy(1, 2).wait_recv()
    mid_unit(far_base)
    part_out(2)
    prod_pair = remote(prod.at[0], prod.at[1], pp_sem.at[0], pp_sem.at[1], me, 1 - core)
    prod_pair.start()
    send_back(2)
    prod_pair.wait()

    def prod_copy(s):
        target = (me + s) % n
        return remote(prod.at[0, target], prod.at[2, me], prod_send.at[s], prod_recv.at[s], target)

    prod[0] = (prod[0] + prod[1]).astype(BF16).astype(F32)
    for s in range(1, n):
        prod_copy(s).start()
    prod[2, me] = prod[0, me]

    eye = lax.broadcasted_iota(jnp.int32, (128, 128), 0) == lax.broadcasted_iota(jnp.int32, (128, 128), 1)

    def lay(column):
        return jnp.sum(jnp.where(eye, column, 0.0), axis=0, keepdims=True)

    @pl.loop(0, 2 * width // 128)
    def _(d):
        span = pl.ds(pl.multiple_of(d * 128, 128), 128)
        x = rows[0, :, :, span].reshape(n * cap, 128)
        sums = lax.dot_general(x, grads[...].reshape(n * cap, 2 * hid), ROWS, preferred_element_type=F32)
        w_in[span, :] = sums.astype(BF16)
        square = sums * sums
        for k in range(2):
            column = sum(
                jnp.sum(square[:, j * 256 + k * 128:j * 256 + k * 128 + 128], axis=1, keepdims=True)
                for j in range(tiles)
            )
            norms[0, k:k + 1, span] = lay(column)

    norm_pair = remote(norms.at[0], norms.at[1], norm_sem.at[0], norm_sem.at[1], me, 1 - core)
    norm_pair.start()
    outs = []
    for j in range(tiles):
        for k, w in enumerate((gate_w, up_w)):
            outs.append(pltpu.make_async_copy(
                w_in.at[:, pl.ds(j * 256 + k * 128, 128)], w.at[0, :, pl.ds(j * 128, 128)], out_sem.at[len(outs)]
            ))
    for out in outs:
        out.start()

    @pl.when(inner)
    def _():
        far_combine(1)

    col_norm[...] = jnp.zeros_like(col_norm)

    @pl.loop(0, 2 * width // step)
    def _(d):
        span = pl.ds(pl.multiple_of(d * step, step), step)
        x = rows[1, :, :, span].reshape(n * cap, step)
        sums = lax.dot_general(
            hidden[...].reshape(n * cap, hid), x, ROWS, preferred_element_type=F32
        )
        w_out[:, span] = sums.astype(BF16)
        col_norm[...] += jnp.sum(sums * sums, axis=1, keepdims=True)

    last = pltpu.make_async_copy(w_out, down_w.at[0], out_sem.at[2 * tiles])
    last.start()
    for j in range(tiles):
        down_norms[:, pl.ds(j * 128, 128)] = jnp.broadcast_to(lay(col_norm[j * 128:(j + 1) * 128]), (8, 128))
    norm_pair.wait()
    in_norms[...] = norms[0] + norms[1]

    for s in range(1, n):
        prod_copy(s).wait_recv()
    table = prod[2][:, 0, :].astype(BF16)
    ids = lax.broadcasted_iota(jnp.int32, (n, rows_t), 0)
    lanes = lax.broadcasted_iota(jnp.int32, (128, rows_t), 0)
    gate_out[...] = jnp.zeros_like(gate_out)
    for k in range(2):
        hit = (meta_ref[4 + k:5 + k, :].astype(jnp.int32) == ids).astype(F32).astype(BF16)
        found = lax.dot_general(table, hit, ROWS, preferred_element_type=F32)
        rank = meta_ref[6 + k:7 + k, :].astype(jnp.int32)
        value = jnp.sum(jnp.where(rank == lanes, found, 0.0), axis=0, keepdims=True)
        gate_out[k:k + 1, :] = value / meta_ref[2 + k:3 + k, :]

    tok_done = []
    for c in range(chunks):
        for s in range(1, half_n):
            other = (spot + s) % half_n
            block = back_own.at[other, :, cols(c)]
            remote(block, block, bo_send.at[c, 0], bo_recv.at[c, other], me, 1 - core).wait_recv()
        mine = combine(0, back_own, c)
        far_part_copy(0, c).wait_recv()
        held[0, 0, :, cols(c)] = (mine + far_part[:, cols(c)].astype(F32)).astype(BF16)
        done = pltpu.make_async_copy(held.at[0, 0, :, cols(c)], tok_out.at[:, cols(c)], tok_sem.at[c])
        done.start()
        tok_done.append(done)

    for a in range(2):
        for slot in range(3):
            pair_copy(a, slot).wait_send()
    for c in range(chunks):
        for kind in range(3):
            part_copy(kind, c).wait_send()
        for s in range(1, half_n):
            back_own_copy(c, s).wait_send()
        for b in range(2):
            for s in range(1, quarter):
                back_far_copy(b, c, s).wait_send()
    for s in range(1, n):
        prod_copy(s).wait_send()

    @pl.when(inner)
    def _():
        near_meta.wait_send()
        pass_meta.wait_send()
        for a in range(2):
            near_copy(a).wait_send()
            for b in range(2):
                for s in range(quarter):
                    far_copy(b, a, s, True).wait_send()
                for s in range(1, quarter):
                    far_copy(b, a, s, False).wait_send()
        for c in range(chunks):
            for b in range(2):
                far_part_copy(b, c).wait_send()

    @pl.when(outer)
    def _():
        relay_meta.wait_send()
        for a in range(2):
            relay_copy(a).wait_send()
        for c in range(chunks):
            for b in range(2):
                back_far_copy(b, c, 0).wait_send()

    for done in tok_done:
        done.wait()
    for out in outs:
        out.wait()
    last.wait()


def scratch(n, cap, rows_t, width, hid):
    half_n, quarter = n // 2, n // 4
    chunks = width // wide(width)
    dma = pltpu.SemaphoreType.DMA
    buffers = [
        ((2, 2, rows_t, width), BF16),
        ((2, rows_t, width), BF16),
        ((2, 8, rows_t), F32),
        ((8, rows_t), F32),
        ((2, 2, half_n, cap, width), BF16),
        ((2, n, cap, 2 * width), BF16),
        ((3, half_n * cap, rows_t), BF16),
        ((3, half_n * cap, 1), F32),
        ((2 * width, 2 * hid), BF16),
        ((hid, 2 * width), BF16),
        ((n, cap, 2 * hid), F32),
        ((n, cap, 2 * hid), BF16),
        ((n, cap, hid), BF16),
        ((n, cap, width), BF16),
        ((n, cap, width), BF16),
        ((half_n, cap, width), BF16),
        ((2, half_n, cap, width), BF16),
        ((rows_t, width), BF16),
        ((3, n, 8, 128), F32),
        ((2, 8, 2 * width), F32),
        ((hid, 1), F32),
    ]
    semaphores = [
        (2, 2), (2, 2), (2,), (2,), (6,),
        (2, half_n), (2, half_n), (2, 2, 2, quarter), (2, 2, quarter), (2, 3), (2, 3), (2 * hid // 128 + 1,),
        (3, chunks), (3, chunks), (chunks, half_n), (chunks, half_n), (2, chunks, quarter), (2, chunks, half_n),
        (2, chunks), (chunks,), (n,), (n,), (2,), (2,), (2 * hid // 128 + 1,), (chunks,),
    ]
    size = 2 * rows_t * width * 2
    for shape, kind in buffers:
        lanes = -(-shape[-1] // 128) * 128
        count = lanes
        for extent in shape[:-1]:
            count *= extent
        size += count * (2 if kind == BF16 else 4)
    return [pltpu.VMEM(*b) for b in buffers] + [dma(s) for s in semaphores], size


def fused(n, cap, tokens, cotangent, meta, w_gate, w_up, w_down):
    rows_t, width = tokens.shape
    hid = w_down.shape[1]
    vm = pl.BlockSpec(memory_space=pltpu.VMEM)
    anywhere = pl.BlockSpec(memory_space=pl.ANY)
    shape = jax.ShapeDtypeStruct
    return pl.pallas_call(
        functools.partial(layer_kernel, n, cap),
        out_shape=(
            shape(tokens.shape, BF16), shape((8, rows_t), F32),
            shape(w_gate.shape, BF16), shape(w_up.shape, BF16), shape(w_down.shape, BF16),
            shape((8, 2 * width), F32), shape((8, hid), F32),
        ),
        in_specs=[vm] * 3 + [anywhere] * 3,
        out_specs=[anywhere, vm, anywhere, anywhere, anywhere, vm, vm],
        scratch_shapes=scratch(n, cap, rows_t, width, hid)[0],
        compiler_params=pltpu.CompilerParams(
            collective_id=0, has_side_effects=True, vmem_limit_bytes=VMEM_BYTES
        ),
        cost_estimate=pl.CostEstimate(flops=10**10, bytes_accessed=10**8, transcendentals=0),
    )(tokens, cotangent, meta, w_gate, w_up, w_down)


def per_device(tokens, cotangent, experts, gate, w_gate, w_up, w_down):
    groups = lax.axis_size("ep")
    tok_rows, top = experts.shape
    cap = 3 * tok_rows * top // (2 * groups)
    cap = (cap + 7) // 8 * 8
    slot = slots_of(experts.T, groups, cap)
    gate_t = gate.T
    rank = slot - experts.T * cap
    meta = jnp.concatenate([slot.astype(F32), gate_t, experts.T.astype(F32), rank.astype(F32)], axis=0)
    tok, gate_grad, gate_w, up_w, down_w, in_norms, down_norms = fused(
        groups, cap, tokens, cotangent, meta, w_gate, w_up, w_down
    )
    return (
        tok, gate_grad[:top].T, gate_w, up_w, down_w, in_norms[0][None], in_norms[1][None], down_norms[0][None],
    )


def plain_device(tokens, cotangent, experts, gate, w_gate, w_up, w_down):
    groups = lax.axis_size("ep")
    tok_rows, top = experts.shape
    cap = 3 * tok_rows * top // (2 * groups)
    total = groups * cap
    half = tokens.shape[1]
    core = lax.axis_index("tp")
    swap = [(0, 1), (1, 0)]
    slot = slots_of(experts.T, groups, cap)
    gate_t = gate.T
    slot_ids = lax.broadcasted_iota(jnp.int32, (total, tok_rows), 0)
    match = [slot[k][None, :] == slot_ids for k in range(top)]
    pick = sum(m.astype(F32) for m in match).astype(BF16)
    slot_gate = sum(
        jnp.sum(jnp.where(m, gate_t[k][None, :], 0.0), axis=1, keepdims=True) for k, m in enumerate(match)
    )
    pick, slot_gate = lax.optimization_barrier((pick, slot_gate))

    def exchange(x):
        y = lax.all_to_all(x.reshape(groups, cap, -1), "ep", split_axis=0, concat_axis=0, tiled=True)
        return y.reshape(total, -1)

    sent_tok = jnp.dot(pick, tokens, preferred_element_type=F32).astype(BF16)
    own_tok = exchange(sent_tok)
    cot = jnp.dot(pick, cotangent, preferred_element_type=F32)
    sent_cot = (cot * slot_gate).astype(BF16)
    own_cot = exchange(sent_cot)

    def both(own, other):
        return jnp.where(
            core == 0,
            jnp.concatenate([own, other], axis=1),
            jnp.concatenate([other, own], axis=1),
        )

    w_in = jnp.concatenate([w_gate[0], w_up[0]], axis=1)
    hid = w_gate.shape[2]
    w_mine = lax.dynamic_slice_in_dim(w_in, core * half, half, 0)
    w_other = lax.dynamic_slice_in_dim(w_in, (1 - core) * half, half, 0)
    d_mine = lax.dynamic_slice_in_dim(w_down[0], core * half, half, 1)
    d_other = lax.dynamic_slice_in_dim(w_down[0], (1 - core) * half, half, 1)

    other_tok = lax.ppermute(own_tok, "tp", swap)
    rows_in = both(own_tok, other_tok)
    pre = jnp.dot(rows_in, w_in, preferred_element_type=F32)
    other_cot = lax.ppermute(own_cot, "tp", swap)
    grad_mine = lax.dot_general(own_cot, d_mine, LAST, preferred_element_type=F32)
    hidden_grad = grad_mine + lax.dot_general(other_cot, d_other, LAST, preferred_element_type=F32)
    gate_pre, up_pre = pre[:, :hid], pre[:, hid:]
    sigma = jax.nn.sigmoid(gate_pre)
    active = gate_pre * sigma
    hidden = (active * up_pre).astype(BF16)
    product_part = jnp.sum(hidden.astype(F32) * hidden_grad, axis=1)
    grads = jnp.concatenate(
        [
            (hidden_grad * up_pre * sigma * (1.0 + gate_pre * (1.0 - sigma))).astype(BF16),
            (hidden_grad * active).astype(BF16),
        ],
        axis=1,
    )
    part_other = lax.dot_general(grads, w_other, LAST, preferred_element_type=F32).astype(BF16)
    arrived = lax.ppermute(part_other, "tp", swap)
    part_mine = lax.dot_general(grads, w_mine, LAST, preferred_element_type=F32)
    row_grads = (part_mine + arrived.astype(F32)).astype(BF16)
    high = product_part.astype(BF16)
    low = (product_part - high.astype(F32)).astype(BF16)
    lane = lax.broadcasted_iota(jnp.int32, (total, 128), 1)
    spare = jnp.where(lane == 0, high[:, None], jnp.where(lane == 1, low[:, None], jnp.zeros((), BF16)))
    row_grads = jnp.concatenate([row_grads, spare], axis=1)
    back = exchange(row_grads)

    rows_in, grads, other_cot, hidden, row_grads = lax.optimization_barrier(
        (rows_in, grads, other_cot, hidden, row_grads)
    )
    gate_sum = lax.dot_general(rows_in, grads[:, :hid], ROWS, preferred_element_type=F32)
    up_sum = lax.dot_general(rows_in, grads[:, hid:], ROWS, preferred_element_type=F32)
    rows_cot = both(own_cot, other_cot)
    down_sum = lax.dot_general(hidden, rows_cot, ROWS, preferred_element_type=F32)
    in_norms = jnp.stack([jnp.sum(gate_sum * gate_sum, axis=1), jnp.sum(up_sum * up_sum, axis=1)])
    down_norms = jnp.sum(down_sum * down_sum, axis=1)
    in_norms = in_norms + lax.ppermute(in_norms, "tp", swap)
    pair = lax.dot_general(
        back[:, half:], jnp.concatenate([match[k] for k in range(top)], axis=1).astype(BF16), ROWS,
        preferred_element_type=F32,
    )
    route_products = (pair[0] + pair[1]).reshape(top, tok_rows)
    route_products = route_products + lax.ppermute(route_products, "tp", swap)
    gate_grad = (route_products.astype(BF16).astype(F32) / gate_t).T
    token_grad = lax.dot_general(pick, back[:, :half], ROWS, preferred_element_type=F32).astype(BF16)
    return (
        token_grad,
        gate_grad,
        gate_sum.astype(BF16)[None],
        up_sum.astype(BF16)[None],
        down_sum.astype(BF16)[None],
        in_norms[0][None],
        in_norms[1][None],
        down_norms[None],
    )


def layer(run, *arrays):
    return run(*arrays)


def fits(n, cores, shapes):
    tokens, experts, w_down = shapes
    rows_t, top = experts[0] // n, experts[1]
    cap = (3 * rows_t * top // (2 * n) + 7) // 8 * 8
    width, hid = tokens[1] // cores, w_down[1] // cores
    if n % 4 or cores != 2 or top != 2 or hid % 128 or width % 128 or cap > 128 or w_down[0] != n:
        return False
    return scratch(n, cap, rows_t, width, hid)[1] < VMEM_BYTES


def solution(mesh):
    placed = (
        P("ep", "tp"),
        P("ep", "tp"),
        P("ep", None),
        P("ep", None),
        P("ep", None, "tp"),
        P("ep", None, "tp"),
        P("ep", "tp", None),
    )

    def mapped(run):
        return jax.shard_map(
            functools.partial(layer, run),
            mesh=mesh,
            in_specs=placed,
            out_specs=(
                P("ep", "tp"),
                P("ep", None),
                P("ep", None, "tp"),
                P("ep", None, "tp"),
                P("ep", "tp", None),
                P("ep", None),
                P("ep", None),
                P("ep", "tp"),
            ),
            check_vma=False,
        )

    plain = mapped(plain_device)
    quick = mapped(per_device)

    def run(*arrays):
        shapes = (arrays[0].shape, arrays[2].shape, arrays[6].shape)
        return (quick if fits(mesh.shape["ep"], mesh.shape["tp"], shapes) else plain)(*arrays)

    return run
```

time: 282 us -> 222 us (0.79)
  the two profiles are of different devices: /device:TPU:15 before, /device:TPU:0 now
where the time goes in v1:
time: 222 us; the launch traced here: 221 us
  Pallas kernels  203 us (91%)
  local copies, waits for them, and re-layouts  13.9 us (6%)
  other arithmetic  3.46 us (2%)
    pallas_call x1, Pallas kernels, fused(): pl.pallas_call(functools.partial(layer_kernel, n, cap), out_shape=(shape(...  203 us
    unnamed x10, local copies, waits for them, and re-layouts  8.8 us

profile of v1, /device:TPU:0, one launch (start us, length us, event | category | flops | bytes accessed | tf_op | source)
XLA Modules:
  0.0 221.2 jit_solution(13111157940658128527)
XLA Ops:
  0.6 0.7 bitcast_convert_fusion
  1.3 0.8 slice_reduce_fusion.1
  2.1 0.2 select_reduce_fusion.1
  2.3 0.8 reshape_add_fusion.1
  3.1 0.7 fusion.3
  3.8 1.3 pad_maximum_fusion.meta_ref
  5.1 203.0 %shard_map.134 = (bf16[384,1536]{1,0:T(8,128)(2,1)}, f32[8,384]{1,0:T(8,128)}, bf16[1,3072,384]{2,1,0:T(8,128)(2,1)}, bf16[1,3072,384]{2,1,0:T(8,128)(2,1)}, bf1...) custom-call(bf16[384,1536]{1,0:T(8,128)(2,1)} %tok_ref.1, bf16[384,1536]{1,0:T(8,128)(2,1)} %cot_ref.1, ...), custom_call_target="tpu_custom_call" | custom-call | flops 10000000000 | bytes 100000000 | tf_op jit(solution)/shard_map/pallas_call | solution.py:560
  208.1 0.0 copy-start.2
  208.1 1.4 slice.25
  209.5 1.3 slice_bitcast_fusion
  210.8 1.6 fusion.4
  212.4 2.4 %copy.19 = bf16[384,1536]{1,0:T(8,128)(2,1)} copy(bf16[384,1536]{1,0:T(8,128)(2,1)} %get-tuple-element.40) | data formatting | bytes 2359296
  214.8 0.0 copy-done.2
  214.8 0.0 copy-start.1
  214.8 1.4 copy.20
  216.2 1.1 copy-done.1
  217.3 0.0 copy-start
  217.3 1.4 copy.21
  218.7 1.1 copy-done
  219.8 1.4 copy.22
  (2 shorter events, 0.0 us)
Async XLA Ops:
  208.1 6.7 %copy-start.2 = (bf16[1,3072,384]{2,1,0:T(8,128)(2,1)S(1)}, bf16[1,3072,384]{2,1,0:T(8,128)(2,1)}, u32[]{:S(2)}) copy-start(bf16[1,3072,384]{2,1,0:T(8,128)(2,1)} %get-tuple-element.42) | copy-start | bytes 7077892
  214.8 2.5 %copy-start.1 = (bf16[1,3072,384]{2,1,0:T(8,128)(2,1)S(1)}, bf16[1,3072,384]{2,1,0:T(8,128)(2,1)}, u32[]{:S(2)}) copy-start(bf16[1,3072,384]{2,1,0:T(8,128)(2,1)} %get-tuple-element.43) | copy-start | bytes 7077892
  217.3 2.5 %copy-start = (bf16[1,384,3072]{2,1,0:T(8,128)(2,1)S(1)}, bf16[1,384,3072]{2,1,0:T(8,128)(2,1)}, u32[]{:S(2)}) copy-start(bf16[1,384,3072]{2,1,0:T(8,128)(2,1)} %get-tuple-element.44) | copy-start | bytes 7077892
